TPU v7x, 128 devices: a whole 4x4x4 slice. The times are simulated.
128 devices in a mesh: sp: 16 (over z, y), tp: 8 (over x, core).
Axes of the slice: x: 4, y: 4, z: 4, core: 2. Of those that a mesh axis runs over, the one named last changes fastest.
Arguments:
- arriving_hidden_sum: bfloat16 [16384, 2048], P('sp'), may hold values from -40 to 40
- content_entries_clustered: bfloat16 [16384, 4096], P('sp', 'tp'), may hold values from -6 to 6
- leaving_switch_entries: bfloat16 [16384, 4096], P('sp', 'tp'), may hold values from -6 to 6
- linked_source_target_pairs: bfloat16 [16384, 8, 2, 128], P('sp', 'tp'), may hold values from -1.78125 to 1.78125
- raw_interval_length: bfloat16 [16384, 64], P('sp', 'tp'), may hold values from -5 to 5
- spike_extra_lognoise: float32 [16384, 64], P('sp', 'tp'), may hold values from -0.6 to 0
- content_filter_kernel: bfloat16 [4, 4096], P(None, 'tp'), may hold values from -3 to 3
- coupling_filter_kernel: bfloat16 [4, 8, 2, 128], P(None, 'tp'), may hold values from -3 to 3
- interval_shift_vector: float32 [64], P('tp'), may hold values from -0.5 to 0.5
- fading_speed_exponent: float32 [64], P('tp'), may hold values from -16 to -2.9
- skip_channel_factor: float32 [64], P('tp'), may hold values from 1 to 10
- cluster_rescale_vector: float32 [4096], P('tp'), may hold values from 0.1 to 1.9
- blender_final_tensor: bfloat16 [4096, 2048], P('tp'), may hold values from -0.09375 to 0.09375
- prelayer_rescale_vector: float32 [2048], replicated, may hold values from 0.1 to 1.9
- switching_linear_tensor: bfloat16 [2048, 5632], P('sp', 'tp'), may hold values from -0.125 to 0.125
- widening_linear_tensor: bfloat16 [2048, 5632], P('sp', 'tp'), may hold values from -0.125 to 0.125
- contracting_linear_tensor: bfloat16 [5632, 2048], P('tp', 'sp'), may hold values from -0.078125 to 0.078125
Outputs:
- residual_out: bfloat16 [16384, 2048], P('sp', 'tp')
All inputs are finite; a program needn't handle non-finite values.
Results may differ from a plain program's by a relative error of at most 0.012.
Values may be sent and summed in bfloat16 or wider, within the bound.
No kernel may reach another device: no remote copies, remote signals or barrier semaphores. Data moves between devices by JAX's collectives and lax.ppermute only.
A program may use at most 128 MiB of HBM per device.

v0:
```python
import jax
import jax.numpy as jnp
from jax import lax
from jax.sharding import Mesh
from jax.sharding import PartitionSpec as P

D = 2048
BLOCK_POSITIONS = 128
SP = ("sp_0", "sp_1")
EPS = 1e-06


def rows_first(arrays, axis, dims):
    turned = [jnp.moveaxis(a, dim, 0) for a, dim in zip(arrays, dims)]
    both = jnp.concatenate([t.reshape(len(t), -1) for t in turned], axis=1)
    out, at, outs = (lax.all_gather(both, axis, axis=0, tiled=True), 0, [])
    for t, dim in zip(turned, dims):
        piece = out[:, at : at + t[0].size].reshape(-1, *t.shape[1:])
        outs.append(jnp.moveaxis(piece, 0, dim))
        at += t[0].size
    return tuple(outs)


def from_behind(block, axis, distance):
    devices = range(lax.axis_size(axis))
    route = [(i - distance, i) for i in devices if i - distance in devices]
    return lax.ppermute(block, axis, route)


def neutral_like(array, identity):
    return jax.tree.map(
        lambda part, zero: jnp.zeros_like(part) + jnp.asarray(zero, part.dtype), array, identity
    )


def entering_2(array, axes, combine, identity):
    before = start = neutral_like(array, identity)
    so_far = array
    for axis in reversed(axes):
        count, place = (lax.axis_size(axis), lax.axis_index(axis))
        pieces = jax.tree.map(
            lambda part, kind: lax.all_gather(part.astype(kind), axis),
            so_far,
            (jnp.bfloat16, jnp.bfloat16),
        )
        inside, so_far = (start, start)
        for k in range(count):
            passed = k < place
            so_far = combine(
                so_far, jax.tree.map(lambda part, own: part[k].astype(own.dtype), pieces, array)
            )
            inside = jax.tree.map(lambda new, old: jnp.where(passed, new, old), so_far, inside)
        before = combine(inside, before)
    return before


def conv_block(values, rims, taps):
    taps_count = taps.shape[0]
    length = values.shape[0]
    padded = jnp.concatenate([rims, values], axis=0).astype(jnp.float32)
    running = jnp.zeros(values.shape, jnp.float32)
    for tap_index in range(taps_count):
        running = running + padded[tap_index : tap_index + length] * taps[tap_index].astype(
            jnp.float32
        )
    return jax.nn.silu(running).astype(jnp.bfloat16)


def combine_states(former, latter):
    return (former[0] * jnp.exp(latter[1])[:, :, None, None] + latter[0], former[1] + latter[1])


def shards(
    arriving_hidden_sum,
    content_entries_clustered,
    leaving_switch_entries,
    linked_source_target_pairs,
    raw_interval_length,
    spike_extra_lognoise,
    content_filter_kernel,
    coupling_filter_kernel,
    interval_shift_vector,
    fading_speed_exponent,
    skip_channel_factor,
    cluster_rescale_vector,
    blender_final_tensor,
    prelayer_rescale_vector,
    switching_linear_tensor,
    widening_linear_tensor,
    contracting_linear_tensor,
):
    whole_gate, whole_up, whole_down = rows_first(
        (switching_linear_tensor, widening_linear_tensor, contracting_linear_tensor), SP, (0, 0, 1)
    )
    length = content_entries_clustered.shape[0]
    heads_per_device = raw_interval_length.shape[1]
    groups_dev = linked_source_target_pairs.shape[1]
    per_group = heads_per_device // groups_dev
    head_size = content_entries_clustered.shape[1] // heads_per_device
    state_size = linked_source_target_pairs.shape[3]
    taps_count = content_filter_kernel.shape[0]
    block_count = length // BLOCK_POSITIONS
    couple_flat = linked_source_target_pairs.reshape(length, -1)
    value_rims, couple_rims = from_behind(
        (
            content_entries_clustered[length - taps_count + 1 :],
            couple_flat[length - taps_count + 1 :],
        ),
        SP,
        1,
    )
    values = conv_block(content_entries_clustered, value_rims, content_filter_kernel)
    coupled = conv_block(
        couple_flat, couple_rims, coupling_filter_kernel.reshape(taps_count, -1)
    ).reshape(length, groups_dev, 2, state_size)
    value_blocks = values.reshape(block_count, BLOCK_POSITIONS, heads_per_device, head_size)
    write_maps = coupled[:, :, 0].reshape(block_count, BLOCK_POSITIONS, groups_dev, state_size)
    read_maps = coupled[:, :, 1].reshape(block_count, BLOCK_POSITIONS, groups_dev, state_size)
    interval_lengths = jax.nn.softplus(
        raw_interval_length.astype(jnp.float32) + interval_shift_vector
    )
    fading_log_factor = (
        -jnp.exp(fading_speed_exponent) * interval_lengths + spike_extra_lognoise
    ).reshape(block_count, BLOCK_POSITIONS, heads_per_device)
    interval_lengths = interval_lengths.reshape(block_count, BLOCK_POSITIONS, heads_per_device)
    cum_log = jnp.cumsum(fading_log_factor, axis=1)
    head_cum = jnp.swapaxes(cum_log, 1, 2)
    log_gap = head_cum[:, :, :, None] - head_cum[:, :, None, :]
    causal = jnp.tril(jnp.ones((BLOCK_POSITIONS, BLOCK_POSITIONS), bool))
    intersection = jnp.einsum(
        "blgn,bsgn->bgls", read_maps, write_maps, preferred_element_type=jnp.float32
    )
    intersection = jnp.repeat(intersection, per_group, axis=1)
    weights = (
        intersection
        * jnp.exp(jnp.where(causal, log_gap, -jnp.inf))
        * jnp.swapaxes(interval_lengths, 1, 2)[:, :, None, :]
    ).astype(jnp.bfloat16)
    within = jnp.einsum(
        "bhls,bshp->blhp", weights, value_blocks, preferred_element_type=jnp.float32
    )
    end_log = cum_log[:, -1]
    scaled = (
        value_blocks * (interval_lengths * jnp.exp(end_log[:, None, :] - cum_log))[..., None]
    ).astype(jnp.bfloat16)
    block_states = jnp.einsum(
        "blgn,blgrp->bgrpn",
        write_maps,
        scaled.reshape(block_count, BLOCK_POSITIONS, groups_dev, per_group, head_size),
        preferred_element_type=jnp.float32,
    )
    end_grouped = end_log.reshape(block_count, groups_dev, per_group)

    def carry_step(carry_state, inputs):
        block_added, block_end = inputs
        return (carry_state * jnp.exp(block_end)[:, :, None, None] + block_added, carry_state)

    zeros_state = jnp.zeros((groups_dev, per_group, head_size, state_size), jnp.float32)
    final_state, entering = lax.scan(carry_step, zeros_state, (block_states, end_grouped))
    read_wide = read_maps.astype(jnp.float32)
    carried = (
        jnp.einsum("blgn,bgrpn->blgrp", read_wide, entering).reshape(
            block_count, BLOCK_POSITIONS, heads_per_device, head_size
        )
        * jnp.exp(cum_log)[..., None]
    )
    device_log = jnp.sum(end_log, axis=0).reshape(groups_dev, per_group)
    incoming, _ = entering_2(
        (final_state, device_log), SP, combine_states, (zeros_state, jnp.zeros_like(device_log))
    )
    prior_log = jnp.cumsum(end_log, axis=0) - end_log
    reach_decay = jnp.exp(cum_log + prior_log[:, None, :])
    arrived = (
        jnp.einsum("blgn,grpn->blgrp", read_wide, incoming).reshape(
            block_count, BLOCK_POSITIONS, heads_per_device, head_size
        )
        * reach_decay[..., None]
    )
    mixer = (within + carried + arrived).reshape(
        length, heads_per_device, head_size
    ) + values.reshape(length, heads_per_device, head_size).astype(
        jnp.float32
    ) * skip_channel_factor[
        None, :, None
    ]
    gated = mixer.reshape(length, heads_per_device * head_size) * jax.nn.silu(
        leaving_switch_entries.astype(jnp.float32)
    )
    grouped = gated.reshape(length, groups_dev, per_group * head_size)
    grouped = grouped * lax.rsqrt(jnp.mean(grouped * grouped, axis=-1, keepdims=True) + EPS)
    mixed_rows = (
        grouped.reshape(length, heads_per_device * head_size) * cluster_rescale_vector
    ).astype(jnp.bfloat16)
    partial_sum = jnp.dot(mixed_rows, blender_final_tensor, preferred_element_type=jnp.float32)
    rounded = lax.optimization_barrier(partial_sum.astype(jnp.bfloat16)).astype(jnp.float32)
    col_count = D // lax.axis_size("tp")
    offset = lax.axis_index("tp") * col_count
    mixer_out = lax.psum(rounded.astype(jnp.bfloat16), "tp").astype(jnp.float32)
    residual_whole = (arriving_hidden_sum.astype(jnp.float32) + mixer_out).astype(jnp.bfloat16)
    squares = residual_whole.astype(jnp.float32)
    normed = (
        squares
        * lax.rsqrt(jnp.mean(squares * squares, axis=-1, keepdims=True) + EPS)
        * prelayer_rescale_vector
    ).astype(jnp.bfloat16)
    residual_mid = lax.dynamic_slice_in_dim(residual_whole, offset, col_count, 1)
    gate_pre = jnp.dot(normed, whole_gate, preferred_element_type=jnp.float32)
    up_pre = jnp.dot(normed, whole_up, preferred_element_type=jnp.float32)
    hidden = (jax.nn.silu(gate_pre) * up_pre).astype(jnp.bfloat16)
    down_terms = jnp.dot(hidden, whole_down, preferred_element_type=jnp.float32)
    down_rounded = lax.optimization_barrier(down_terms.astype(jnp.bfloat16)).astype(jnp.float32)
    mlp_cols = lax.psum_scatter(
        down_rounded.astype(jnp.bfloat16), "tp", scatter_dimension=1, tiled=True
    ).astype(jnp.float32)
    return (residual_mid.astype(jnp.float32) + 0.5 * mlp_cols).astype(jnp.bfloat16)


def solution(mesh):
    torus = Mesh(mesh.devices.reshape(4, 4, mesh.shape["tp"]), ("sp_0", "sp_1", "tp"))
    return jax.shard_map(
        shards,
        mesh=torus,
        in_specs=(
            P(SP, None),
            P(SP, "tp"),
            P(SP, "tp"),
            P(SP, "tp", None, None),
            P(SP, "tp"),
            P(SP, "tp"),
            P(None, "tp"),
            P(None, "tp", None, None),
            P("tp"),
            P("tp"),
            P("tp"),
            P("tp"),
            P("tp", None),
            P(),
            P(SP, "tp"),
            P(SP, "tp"),
            P("tp", SP),
        ),
        out_specs=P(SP, "tp"),
        check_vma=False,
    )
```

profile of v0, /device:TPU:0, one launch (start us, length us, event | category | flops | bytes accessed | tf_op | source)
XLA Modules:
  0.0 283.2 jit_solution(7769426850520135814)
XLA Ops:
  9.0 4.2 %collective-permute-start.1 = (bf16[3,256]{0,1:T(8,128)(2,1)}, bf16[3,256]{0,1:T(8,128)(2,1)}, u32[]{:S(2)}, u32[]{:S(2)}) collective-permute-start(bf16[3,256]{0,1:T(8,128)(2,1)} %bitcast.4), channel_id=1, source_target_pairs={{0,8},{8,16},{16,24},{24,32},{32,40},{40,48},{48,56},{56,64},{64,7... | collective-permute-start | bytes 4616 | tf_op jit(solution)/shard_map/ppermute | solution.py:27
  14.7 2.9 %collective-permute-start = (bf16[3,512]{0,1:T(8,128)(2,1)}, bf16[3,512]{0,1:T(8,128)(2,1)S(1)}, u32[]{:S(2)}, u32[]{:S(2)}) collective-permute-start(bf16[3,512]{0,1:T(8,128)(2,1)} %copy.50), channel_id=1, source_target_pairs={{0,8},{8,16},{16,24},{24,32},{32,40},{40,48},{48,56},{56,64},{64,7... | collective-permute-start | bytes 9224 | tf_op jit(solution)/shard_map/ppermute | solution.py:27
  18.2 1.3 bitcast_convert_fusion.3
  20.4 1.5 fusion.102
  25.9 10.7 %all-reduce = bf16[32]{0:T(256)(128)(2,1)S(1)} all-reduce(bf16[32]{0:T(256)(128)(2,1)S(1)} %dynamic-update-slice), channel_id=2, replica_groups=mesh['sp_0'=4,'sp_1'=4,'tp'=8] {'sp_1'}, use_global_device_ids=true, to_apply=%add | all-reduce | flops 32 | bytes 128
  36.7 9.3 %all_gather.22 = bf16[4,1,8]{2,1,0:T(2,128)(2,1)S(1)} all-gather(bf16[1,1,8]{2,1,0:T(2,128)(2,1)S(1)} %get-tuple-element.82), channel_id=1, replica_groups=mesh['sp_0'=4,'sp_1'=4,'tp'=8] {'sp_0'}, dimensions={0}, use_global_device_ids=true | all-gather | bytes 80 | tf_op jit(solution)/shard_map/all_gather | solution.py:42
  49.1 2.0 copy.53
  51.1 2.3 copy.51
  54.9 1.5 copy.69
  56.4 1.8 copy.65
  58.2 1.8 copy.67
  60.0 1.8 copy.61
  61.8 1.3 maximum_convert_fusion.1
  63.1 1.8 multiply_convert_fusion.7
  65.8 1.8 copy.55
  67.6 1.8 copy.54
  69.4 2.1 fusion.108
  71.5 1.8 maximum_convert_fusion
  73.3 2.2 fusion.116
  76.5 1.8 convolution_bitcast_fusion
  78.3 19.0 %while.13 = (s32[]{:T(128)}, f32[1,8,64,128]{3,2,1,0:T(8,128)S(1)}, bf16[8,1,8,64,128]{4,3,2,1,0:T(8,128)(2,1)}, f32[8,1,8]{2,1,0:T(1,128)}, f32[8,1,8,64,128]{4,3,2,1,0:T(8,128)}, /*index=5*/s32[]{:T(128)}, s32[]{:T(128)}) while((s32[]{:T(128)}, f32[1,8,64,128]{3,2,1,0:T(8,128)S(1)}, bf16[8,1,8,64,128]{4,3,2,1,0:T(8,128)(2,1)}, ...), condition=%wide.region_2.3_spmd.clone, body=%wide.region_1.2_spmd.clone.sunk | while | flops 262147 | bytes 1179852 | solution.py:159
  97.3 12.9 %all-gather.1 = bf16[4,8,64,128]{3,2,1,0:T(8,128)(2,1)S(1)} all-gather(bf16[1,8,64,128]{3,2,1,0:T(8,128)(2,1)S(1)} %convert_element_type.347), channel_id=3, replica_groups=mesh['sp_0'=4,'sp_1'=4,'tp'=8] {'sp_1'}, dimensions={0}, use_global_device_ids=true | all-gather | bytes 655360 | tf_op jit(solution)/shard_map/all_gather | solution.py:42
  110.5 13.1 %all_gather.25 = bf16[4,1,8,64,128]{4,3,2,1,0:T(8,128)(2,1)S(1)} all-gather(bf16[1,1,8,64,128]{4,3,2,1,0:T(8,128)(2,1)S(1)} %fusion.66), channel_id=1, replica_groups=mesh['sp_0'=4,'sp_1'=4,'tp'=8] {'sp_0'}, dimensions={0}, use_global_device_ids=true | all-gather | bytes 655360 | tf_op jit(solution)/shard_map/all_gather | solution.py:42
  124.2 1.6 fusion.10
  128.4 2.9 %multiply_reduce_fusion = (f32[1024]{0:T(1024)S(1)}, f32[1024,512]{0,1:T(8,128)S(1)}) fusion(bf16[1024,512]{0,1:T(8,128)(2,1)S(1)} %copy.69, f32[512]{0:T(512)S(1)} %copy-done.20, f32[64,8,8,128]{3,2,1,0:T(8,128)S(1)} %bitcast.152, f32[512]{0:T(512)S(1)} %bitcast.169, f32[1027,512]{0,1:T(8,128)S(1)} %copy-done.3, f32[512]{0:T(512)S(1)} %bitcast.171, ...), kind=kLoop, calls=%fused_computation.42 | loop fusion | flops 12057600 | bytes 13645824 | tf_op jit(solution)/shard_map/reduce_sum | solution.py:190
  131.3 4.5 %convolution_convert_fusion.1 = bf16[1024,2048]{1,0:T(8,128)(2,1)} fusion(bf16[512,2048]{1,0:T(8,128)(2,1)S(1)} %copy-done, f32[1024,512]{0,1:T(8,128)S(1)} %get-tuple-element.81, f32[512]{0:T(512)S(1)} %copy-done.32, f32[1024]{0:T(1024)S(1)} %add_rsqrt_fusion.1), kind=kOutput, calls=%fused_computation.13 | convolution fusion | flops 2151153664 | bytes 8394752 | tf_op jit(solution)/shard_map/dot_general | solution.py:194
  138.1 69.1 %all-reduce.3.cloned.1.call-done = bf16[1024,2048]{1,0:T(8,128)(2,1)} async-done(((bf16[1024,2048]{1,0:T(8,128)(2,1)}), bf16[1024,2048]{1,0:T(8,128)(2,1)}) %all-reduce.3.cloned.1.call-update) | async-done | bytes 4194320 | tf_op jit(solution)/shard_map/psum | solution.py:198
  207.2 7.5 %fusion.2 = (f32[1024]{0:T(1024)S(1)}, bf16[1024,2048]{1,0:T(8,128)(2,1)}) fusion(bf16[1024,2048]{1,0:T(8,128)(2,1)} %all-reduce.3.cloned.1.call-done, bf16[1024,2048]{1,0:T(8,128)(2,1)} %param.19), kind=kLoop, calls=%fused_computation.7 | loop fusion | flops 14679040 | bytes 12587008 | tf_op jit(solution)/shard_map/reduce_sum | solution.py:203
  214.9 7.9 %fusion.8 = f32[1024,704]{0,1:T(8,128)} fusion(bf16[2048,2112]{0,1:T(8,128)(2,1)} %all-gather.4.cloned.1.call-done, bf16[1024,2048]{1,0:T(8,128)(2,1)} %get-tuple-element.79, f32[2048]{0:T(1024)S(1)} %copy-done.31, f32[1024]{0:T(1024)S(1)} %add_rsqrt_fusion), kind=kOutput, calls=%fused_computation.17 | convolution fusion | flops 2961178624 | bytes 9973760 | tf_op jit(solution)/shard_map/dot_general | solution.py:207
  222.8 12.4 %convolution_convert_fusion = bf16[1024,2048]{1,0:T(8,128)(2,1)} fusion(bf16[2048,2112]{0,1:T(8,128)(2,1)} %all-gather.4.cloned.1.call-done, f32[1024,704]{0,1:T(8,128)} %fusion.8, bf16[1024,2048]{1,0:T(8,128)(2,1)} %get-tuple-element.79, f32[2048]{0:T(1024)S(1)} %copy-done.31, f32[1024]{0:T(1024)S(1)} %add_rsqrt_fusion), kind=kOutput, calls=%fused_computation.12 | convolution fusion | flops 5920391168 | bytes 17051648 | tf_op jit(solution)/shard_map/dot_general | solution.py:210
  235.3 38.4 %reduce-scatter.2.cloned.1.call-done = bf16[1024,256]{1,0:T(8,128)(2,1)} async-done(((bf16[1024,2048]{1,0:T(8,128)(2,1)}), bf16[1024,256]{1,0:T(8,128)(2,1)}) %reduce-scatter.2.cloned.1.call-update) | async-done | bytes 524304 | tf_op jit(solution)/shard_map/reduce_scatter | solution.py:212
  273.6 2.2 add_convert_fusion.1
  (137 shorter events, 38.9 us)
Async XLA Ops:
  7.4 123.9 %copy-start = (bf16[512,2048]{1,0:T(8,128)(2,1)S(1)}, bf16[512,2048]{1,0:T(8,128)(2,1)}, u32[]{:S(2)}) copy-start(bf16[512,2048]{1,0:T(8,128)(2,1)} %param.31) | copy-start | bytes 6291460
  7.4 17.0 %copy-start.33 = (u32[128]{0:T(128)S(1)}, u32[128]{0:T(128)}, u32[]{:S(2)}) copy-start(u32[128]{0:T(128)} %constant.76) | copy-start | bytes 1540
  7.4 199.9 %all-reduce.3.cloned.1.call-start = ((), (), s32[]{:S(2)}) async-start(), calls=%async_computation.1 | async-start | bytes 8388608 | tf_op jit(solution)/shard_map/psum | solution.py:198
  9.0 52.9 %collective-permute-start.1 = (bf16[3,256]{0,1:T(8,128)(2,1)}, bf16[3,256]{0,1:T(8,128)(2,1)}, u32[]{:S(2)}, u32[]{:S(2)}) collective-permute-start(bf16[3,256]{0,1:T(8,128)(2,1)} %bitcast.4), channel_id=1, source_target_pairs={{0,8},{8,16},{16,24},{24,32},{32,40},{40,48},{48,56},{56,64},{64,7... | collective-permute-start | bytes 4616 | tf_op jit(solution)/shard_map/ppermute | solution.py:27
  14.7 56.8 %collective-permute-start = (bf16[3,512]{0,1:T(8,128)(2,1)}, bf16[3,512]{0,1:T(8,128)(2,1)S(1)}, u32[]{:S(2)}, u32[]{:S(2)}) collective-permute-start(bf16[3,512]{0,1:T(8,128)(2,1)} %copy.50), channel_id=1, source_target_pairs={{0,8},{8,16},{16,24},{24,32},{32,40},{40,48},{48,56},{56,64},{64,7... | collective-permute-start | bytes 9224 | tf_op jit(solution)/shard_map/ppermute | solution.py:27
  47.8 5.6 %copy-start.30 = (f32[8]{0:T(128)S(1)}, f32[8]{0:T(128)}, u32[]{:S(2)}) copy-start(f32[8]{0:T(128)} %param.29) | copy-start | bytes 100
  73.3 2.2 copy-start.2
  75.8 2.5 copy-start.4
  78.3 32.0 %copy-start.21 = (f32[8]{0:T(128)S(1)}, f32[8]{0:T(128)}, u32[]{:S(2)}) copy-start(f32[8]{0:T(128)} %get-tuple-element.108) | copy-start | bytes 100
  78.3 32.0 %copy-start.22 = (f32[8]{0:T(128)S(1)}, f32[8]{0:T(128)}, u32[]{:S(2)}) copy-start(f32[8]{0:T(128)} %get-tuple-element.109) | copy-start | bytes 100
  78.3 32.0 %copy-start.23 = (f32[8]{0:T(128)S(1)}, f32[8]{0:T(128)}, u32[]{:S(2)}) copy-start(f32[8]{0:T(128)} %get-tuple-element.110) | copy-start | bytes 100
  78.3 32.0 %copy-start.24 = (f32[8]{0:T(128)S(1)}, f32[8]{0:T(128)}, u32[]{:S(2)}) copy-start(f32[8]{0:T(128)} %get-tuple-element.111) | copy-start | bytes 100
  97.3 26.4 %copy-start.6 = (bf16[1024,1,1,128]{3,0,2,1:T(8,128)(2,1)S(1)}, bf16[1024,1,1,128]{3,0,2,1:T(8,128)(2,1)}, u32[]{:S(2)}) copy-start(bf16[1024,1,1,128]{3,0,2,1:T(8,128)(2,1)} %copy.54) | copy-start | bytes 786436
  97.3 26.3 %copy-start.8 = (bf16[8,1,8,64,128]{4,3,2,1,0:T(8,128)(2,1)S(1)}, bf16[8,1,8,64,128]{4,3,2,1,0:T(8,128)(2,1)}, u32[]{:S(2)}) copy-start(bf16[8,1,8,64,128]{4,3,2,1,0:T(8,128)(2,1)} %get-tuple-element.33) | copy-start | bytes 3145732
  110.5 13.6 %copy-start.5 = (bf16[64,8,8,128]{3,2,1,0:T(8,128)(2,1)S(1)}, bf16[64,8,8,128]{3,2,1,0:T(8,128)(2,1)}, u32[]{:S(2)}) copy-start(bf16[64,8,8,128]{3,2,1,0:T(8,128)(2,1)} %copy-done.4) | copy-start | bytes 3145732
  110.5 13.6 %copy-start.9 = (f32[8,128,128]{2,1,0:T(8,128)S(1)}, f32[8,128,128]{2,1,0:T(8,128)}, u32[]{:S(2)}) copy-start(f32[8,128,128]{2,1,0:T(8,128)} %fusion.108) | copy-start | bytes 1572868
  110.5 13.6 %copy-start.16 = (f32[8,8,128]{2,1,0:T(8,128)S(1)}, f32[8,8,128]{2,1,0:T(8,128)}, u32[]{:S(2)}) copy-start(f32[8,8,128]{2,1,0:T(8,128)} %copy.57) | copy-start | bytes 98308
  110.5 13.6 %copy-start.17 = (f32[8,8,128]{2,1,0:T(8,128)S(1)}, f32[8,8,128]{2,1,0:T(8,128)}, u32[]{:S(2)}) copy-start(f32[8,8,128]{2,1,0:T(8,128)} %get-tuple-element.92) | copy-start | bytes 98308
  110.5 13.6 %copy-start.18 = (pred[128,128]{1,0:T(8,128)(4,1)S(1)}, pred[128,128]{1,0:T(8,128)(4,1)}, u32[]{:S(2)}) copy-start(pred[128,128]{1,0:T(8,128)(4,1)} %iota_compare_fusion) | copy-start | bytes 49156
  124.1 1.7 copy-start.13
  124.1 1.7 copy-start.14
  124.2 1.7 copy-start.25
  124.2 1.7 copy-start.26
  124.2 1.7 copy-start.27
  124.2 1.7 copy-start.28
  124.2 1.7 copy-start.29
  126.7 1.7 copy-start.3
  128.4 2.9 %copy-start.32 = (f32[512]{0:T(512)S(1)}, f32[512]{0:T(512)}, u32[]{:S(2)}) copy-start(f32[512]{0:T(512)} %param.30) | copy-start | bytes 6148
  135.9 79.1 %all-gather.4.cloned.1.call-start = ((), (), s32[]{:S(2)}) async-start(), calls=%async_computation.2 | async-start | bytes 9191424 | tf_op jit(solution)/shard_map/all_gather | solution.py:16
  137.8 77.1 %copy-start.31 = (f32[2048]{0:T(1024)S(1)}, f32[2048]{0:T(1024)}, u32[]{:S(2)}) copy-start(f32[2048]{0:T(1024)} %param.32) | copy-start | bytes 24580
  137.8 135.8 %reduce-scatter.2.cloned.1.call-start = ((), (), s32[]{:S(2)}) async-start(), calls=%async_computation.3 | async-start | bytes 4718592 | tf_op jit(solution)/shard_map/reduce_scatter | solution.py:212
  235.2 40.6 %copy-start.1 = (bf16[512,2048]{1,0:T(8,128)(2,1)S(1)}, bf16[512,2048]{1,0:T(8,128)(2,1)}, u32[]{:S(2)}) copy-start(bf16[512,2048]{1,0:T(8,128)(2,1)} %param.31) | copy-start | bytes 6291460
  (7 other events, 7.7 us)
Sparse Core Ops, SparseCore 0:
  136.0 71.1 all-reduce.2
  235.4 38.2 reduce-scatter.1
Sparse Core Ops, SparseCore 1:
  138.5 76.4 all-gather.3
where the time goes:
time: 284 us; the launch traced here: 283 us
  waiting for transfers between devices  108 us (38%)
  blocking collectives  46 us (16%)
  other arithmetic  43.5 us (15%)
  matrix products  31.6 us (11%)
  local copies, waits for them, and re-layouts  30.9 us (11%)
  between operations  16 us (6%)
  starting transfers between devices  7.38 us (3%)
    psum x1, waiting for transfers between devices, shards(): mixer_out = lax.psum(rounded.astype(jnp.bfloat16), 'tp').astype(jnp.float32)  69.1 us
    reduce_scatter x1, waiting for transfers between devices, shards(): lax.psum_scatter(down_rounded.astype(jnp.bfloat16), 'tp', scatter_dimensi...  38.4 us
    all_gather x3, blocking collectives, entering_2(): lax.all_gather(part.astype(kind), axis)  35.3 us
    dot_general x1, matrix products, shards(): down_terms = jnp.dot(hidden, whole_down, preferred_element_type=jnp.float32)  12.4 us
    unnamed x1, blocking collectives  10.7 us
    unnamed x75, local copies, waits for them, and re-layouts  8.9 us
    add x8, other arithmetic, carry_step(): carry_state * jnp.exp(block_end)[:, :, None, None] + block_added  8.32 us
    dot_general x1, matrix products, shards(): gate_pre = jnp.dot(normed, whole_gate, preferred_element_type=jnp.float32)  7.9 us
  transfers between devices with their start and end apart: 5, of which 3 were waited for; matrix products, arithmetic and copies ran while one was open for 15% of the time, Pallas kernels for 0%

commit v1 on v0

--- a/solution.py
+++ b/solution.py
@@ -195,7 +195,9 @@
     rounded = lax.optimization_barrier(partial_sum.astype(jnp.bfloat16)).astype(jnp.float32)
     col_count = D // lax.axis_size("tp")
     offset = lax.axis_index("tp") * col_count
-    mixer_out = lax.psum(rounded.astype(jnp.bfloat16), "tp").astype(jnp.float32)
+    mixer_out = jnp.sum(lax.all_gather(rounded.astype(jnp.bfloat16), "tp"), axis=0).astype(
+        jnp.float32
+    )
     residual_whole = (arriving_hidden_sum.astype(jnp.float32) + mixer_out).astype(jnp.bfloat16)
     squares = residual_whole.astype(jnp.float32)
     normed = (

time: 284 us -> 460 us (1.62)
  waiting for transfers between devices: 108 us -> 249 us
  other arithmetic: 43.5 us -> 78.2 us
    all_gather x0 -> x1, waiting for transfers between devices: none -> 152 us  [shards(): lax.all_gather(rounded.astype(jnp.bfloat16), 'tp')]
    psum x1 -> x0, waiting for transfers between devices: 69.1 us -> none  [shards(): mixer_out = lax.psum(rounded.astype(jnp.bfloat16), 'tp').astype(jnp.float32)]
    all_gather x1, waiting for transfers between devices: 0.16 us -> 60.1 us  [rows_first(): out, at, outs = (lax.all_gather(both, axis, axis=0, tiled=True), 0, [])]
    another operation x1, other arithmetic: 1.18 us -> 23.3 us  [shards(): cum_log = jnp.cumsum(fading_log_factor, axis=1)]
    reduce_sum x0 -> x1, other arithmetic: none -> 14.2 us  [shards(): jnp.sum(lax.all_gather(rounded.astype(jnp.bfloat16), 'tp'), axis=0)]
    unnamed x75 -> x79, local copies, waits for them, and re-layouts: 8.9 us -> 9.54 us
  transfers between devices with their start and end apart: 5 -> 5, of which waited for: 3 -> 3; matrix products, arithmetic and copies ran while one was open for 15% -> 17% of each run, Pallas kernels for 0% -> 0%
where the time goes in v1:
time: 460 us; the launch traced here: 459 us
  waiting for transfers between devices  249 us (54%)
  other arithmetic  78.2 us (17%)
  blocking collectives  45.4 us (10%)
  local copies, waits for them, and re-layouts  31.8 us (7%)
  matrix products  31.7 us (7%)
  between operations  14.3 us (3%)
  starting transfers between devices  8.01 us (2%)
    all_gather x1, waiting for transfers between devices, shards(): lax.all_gather(rounded.astype(jnp.bfloat16), 'tp')  152 us
    all_gather x1, waiting for transfers between devices, rows_first(): out, at, outs = (lax.all_gather(both, axis, axis=0, tiled=True), 0, [])  60.1 us
    reduce_scatter x1, waiting for transfers between devices, shards(): lax.psum_scatter(down_rounded.astype(jnp.bfloat16), 'tp', scatter_dimensi...  37.2 us
    all_gather x3, blocking collectives, entering_2(): lax.all_gather(part.astype(kind), axis)  35.3 us
    another operation x1, other arithmetic, shards(): cum_log = jnp.cumsum(fading_log_factor, axis=1)  23.3 us
    reduce_sum x1, other arithmetic, shards(): jnp.sum(lax.all_gather(rounded.astype(jnp.bfloat16), 'tp'), axis=0)  14.2 us
    dot_general x1, matrix products, shards(): down_terms = jnp.dot(hidden, whole_down, preferred_element_type=jnp.float32)  12.5 us
    unnamed x1, blocking collectives  10.1 us
  transfers between devices with their start and end apart: 5, of which 3 were waited for; matrix products, arithmetic and copies ran while one was open for 17% of the time, Pallas kernels for 0%

profile of v1, /device:TPU:0, one launch (start us, length us, event | category | flops | bytes accessed | tf_op | source)
XLA Modules:
  0.0 458.7 jit_solution(16379918566008575677)
XLA Ops:
  8.2 3.6 collective-permute-start
  13.3 4.1 collective-permute-start.1
  18.0 1.5 fusion.102
  19.7 23.3 %fusion.107 = f32[8,128,8]{2,0,1:T(8,128)S(1)} fusion(f32[8,128,8]{2,0,1:T(8,128)S(1)} %copy.56), kind=kOutput, calls=%fused_computation.174 | output fusion | flops 1040384 | bytes 65536 | tf_op jit(solution)/shard_map/jit(cumsum)/reduce_window_sum | solution.py:126
  46.1 10.1 %all-reduce = bf16[32]{0:T(256)(128)(2,1)S(1)} all-reduce(bf16[32]{0:T(256)(128)(2,1)S(1)} %dynamic-update-slice), channel_id=2, replica_groups=mesh['sp_0'=4,'sp_1'=4,'tp'=8] {'sp_1'}, use_global_device_ids=true, to_apply=%add | all-reduce | flops 32 | bytes 128
  56.3 9.3 %all_gather.28 = bf16[4,1,8]{2,1,0:T(2,128)(2,1)S(1)} all-gather(bf16[1,1,8]{2,1,0:T(2,128)(2,1)S(1)} %get-tuple-element.82), channel_id=1, replica_groups=mesh['sp_0'=4,'sp_1'=4,'tp'=8] {'sp_0'}, dimensions={0}, use_global_device_ids=true | all-gather | bytes 80 | tf_op jit(solution)/shard_map/all_gather | solution.py:42
  68.6 2.3 copy.51
  71.0 2.0 copy.53
  73.0 1.8 copy.61
  75.6 1.8 copy.65
  78.2 1.5 copy.69
  83.7 1.8 multiply_convert_fusion.7
  86.3 1.8 copy.55
  88.1 1.8 copy.54
  89.9 2.1 fusion.108
  92.0 1.8 maximum_convert_fusion
  93.8 2.2 fusion.116
  97.1 1.8 convolution_bitcast_fusion
  98.9 19.1 %while.13 = (s32[]{:T(128)}, f32[1,8,64,128]{3,2,1,0:T(8,128)S(1)}, bf16[8,1,8,64,128]{4,3,2,1,0:T(8,128)(2,1)}, f32[8,1,8]{2,1,0:T(1,128)}, f32[8,1,8,64,128]{4,3,2,1,0:T(8,128)}, /*index=5*/s32[]{:T(128)}, s32[]{:T(128)}) while((s32[]{:T(128)}, f32[1,8,64,128]{3,2,1,0:T(8,128)S(1)}, bf16[8,1,8,64,128]{4,3,2,1,0:T(8,128)(2,1)}, ...), condition=%wide.region_2.3_spmd.clone, body=%wide.region_1.2_spmd.clone.sunk | while | flops 262147 | bytes 1180352 | solution.py:159
  118.0 12.9 %all-gather.1 = bf16[4,8,64,128]{3,2,1,0:T(8,128)(2,1)S(1)} all-gather(bf16[1,8,64,128]{3,2,1,0:T(8,128)(2,1)S(1)} %convert_element_type.349), channel_id=3, replica_groups=mesh['sp_0'=4,'sp_1'=4,'tp'=8] {'sp_1'}, dimensions={0}, use_global_device_ids=true | all-gather | bytes 655360 | tf_op jit(solution)/shard_map/all_gather | solution.py:42
  131.2 13.1 %all_gather.31 = bf16[4,1,8,64,128]{4,3,2,1,0:T(8,128)(2,1)S(1)} all-gather(bf16[1,1,8,64,128]{4,3,2,1,0:T(8,128)(2,1)S(1)} %fusion.66), channel_id=1, replica_groups=mesh['sp_0'=4,'sp_1'=4,'tp'=8] {'sp_0'}, dimensions={0}, use_global_device_ids=true | all-gather | bytes 655360 | tf_op jit(solution)/shard_map/all_gather | solution.py:42
  144.9 1.6 fusion.10
  149.1 2.9 multiply_reduce_fusion
  152.0 4.5 convolution_convert_fusion.1
  158.7 151.9 %all-gather.8.cloned.1.call-done = bf16[8192,2048]{1,0:T(8,128)(2,1)} async-done(((bf16[1024,2048]{1,0:T(8,128)(2,1)}), bf16[8192,2048]{1,0:T(8,128)(2,1)}) %all-gather.8.cloned.1.call-update) | async-done | bytes 33554448 | tf_op jit(solution)/shard_map/all_gather | solution.py:198
  310.5 14.2 %reduce_sum.41 = bf16[1024,2048]{1,0:T(8,128)(2,1)} reduce(bf16[8,1024,2048]{2,1,0:T(8,128)(2,1)} %bitcast.153, bf16[]{:T(256)} %constant.68.clone.1), dimensions={0}, to_apply=%region_6.7 | reduce | flops 14680064 | bytes 37748736 | tf_op jit(solution)/shard_map/reduce_sum | solution.py:198
  324.7 7.5 %fusion.2 = (f32[1024]{0:T(1024)S(1)}, bf16[1024,2048]{1,0:T(8,128)(2,1)}) fusion(bf16[1024,2048]{1,0:T(8,128)(2,1)} %reduce_sum.41, bf16[1024,2048]{1,0:T(8,128)(2,1)} %param.19), kind=kLoop, calls=%fused_computation.7 | loop fusion | flops 14679040 | bytes 12587008 | tf_op jit(solution)/shard_map/reduce_sum | solution.py:205
  332.2 60.1 %all-gather.6.cloned.1.call-done = bf16[2048,2112]{0,1:T(8,128)(2,1)} async-done(((bf16[128,2112]{0,1:T(8,128)(2,1)}), bf16[2048,2112]{0,1:T(8,128)(2,1)}) %all-gather.6.cloned.1.call-update) | async-done | bytes 8650768 | tf_op jit(solution)/shard_map/all_gather | solution.py:16
  392.3 8.0 %fusion.8 = f32[1024,704]{0,1:T(8,128)} fusion(bf16[2048,2112]{0,1:T(8,128)(2,1)} %all-gather.6.cloned.1.call-done, bf16[1024,2048]{1,0:T(8,128)(2,1)} %get-tuple-element.79, f32[2048]{0:T(1024)S(1)} %copy-done.33, f32[1024]{0:T(1024)S(1)} %add_rsqrt_fusion), kind=kOutput, calls=%fused_computation.17 | convolution fusion | flops 2961178624 | bytes 9973760 | tf_op jit(solution)/shard_map/dot_general | solution.py:209
  400.3 12.5 %convolution_convert_fusion = bf16[1024,2048]{1,0:T(8,128)(2,1)} fusion(bf16[2048,2112]{0,1:T(8,128)(2,1)} %all-gather.6.cloned.1.call-done, f32[1024,704]{0,1:T(8,128)} %fusion.8, bf16[1024,2048]{1,0:T(8,128)(2,1)} %get-tuple-element.79, f32[2048]{0:T(1024)S(1)} %copy-done.33, f32[1024]{0:T(1024)S(1)} %add_rsqrt_fusion), kind=kOutput, calls=%fused_computation.12 | convolution fusion | flops 5920391168 | bytes 17051648 | tf_op jit(solution)/shard_map/dot_general | solution.py:212
  412.8 37.2 %reduce-scatter.2.cloned.1.call-done = bf16[1024,256]{1,0:T(8,128)(2,1)} async-done(((bf16[1024,2048]{1,0:T(8,128)(2,1)}), bf16[1024,256]{1,0:T(8,128)(2,1)}) %reduce-scatter.2.cloned.1.call-update) | async-done | bytes 524304 | tf_op jit(solution)/shard_map/reduce_scatter | solution.py:214
  450.0 2.2 add_convert_fusion.1
  (142 shorter events, 41.2 us)
Async XLA Ops:
  6.5 145.4 %copy-start = (bf16[512,2048]{1,0:T(8,128)(2,1)S(1)}, bf16[512,2048]{1,0:T(8,128)(2,1)}, u32[]{:S(2)}) copy-start(bf16[512,2048]{1,0:T(8,128)(2,1)} %param.31) | copy-start | bytes 6291460
  6.5 38.0 %copy-start.35 = (u32[128]{0:T(128)S(1)}, u32[128]{0:T(128)}, u32[]{:S(2)}) copy-start(u32[128]{0:T(128)} %constant.78) | copy-start | bytes 1540
  6.5 37.4 %copy-start.20 = (bf16[4,512]{1,0:T(4,128)(2,1)S(1)}, bf16[4,512]{1,0:T(4,128)(2,1)}, u32[]{:S(2)}) copy-start(bf16[4,512]{1,0:T(4,128)(2,1)} %param.25) | copy-start | bytes 12292
  6.5 37.4 %copy-start.32 = (bf16[4,1,2,128]{3,2,1,0:T(2,128)(2,1)S(1)}, bf16[4,1,2,128]{3,2,1,0:T(2,128)(2,1)}, u32[]{:S(2)}) copy-start(bf16[4,1,2,128]{3,2,1,0:T(2,128)(2,1)} %param.26) | copy-start | bytes 6148
  6.5 304.0 %all-gather.8.cloned.1.call-start = ((), (), s32[]{:S(2)}) async-start(), calls=%async_computation.3 | async-start | bytes 37748736 | tf_op jit(solution)/shard_map/all_gather | solution.py:198
  8.2 83.8 %collective-permute-start = (bf16[3,512]{0,1:T(8,128)(2,1)}, bf16[3,512]{0,1:T(8,128)(2,1)S(1)}, u32[]{:S(2)}, u32[]{:S(2)}) collective-permute-start(bf16[3,512]{0,1:T(8,128)(2,1)} %copy.50), channel_id=1, source_target_pairs={{0,8},{8,16},{16,24},{24,32},{32,40},{40,48},{48,56},{56,64},{64,7... | collective-permute-start | bytes 9224 | tf_op jit(solution)/shard_map/ppermute | solution.py:27
  13.3 69.1 %collective-permute-start.1 = (bf16[3,256]{0,1:T(8,128)(2,1)}, bf16[3,256]{0,1:T(8,128)(2,1)}, u32[]{:S(2)}, u32[]{:S(2)}) collective-permute-start(bf16[3,256]{0,1:T(8,128)(2,1)} %bitcast.4), channel_id=1, source_target_pairs={{0,8},{8,16},{16,24},{24,32},{32,40},{40,48},{48,56},{56,64},{64,7... | collective-permute-start | bytes 4616 | tf_op jit(solution)/shard_map/ppermute | solution.py:27
  68.6 8.8 %copy-start.8 = (f32[8,128,8]{2,0,1:T(8,128)S(1)}, f32[8,128,8]{2,0,1:T(8,128)}, u32[]{:S(2)}) copy-start(f32[8,128,8]{2,0,1:T(8,128)} %get-tuple-element.88) | copy-start | bytes 98308
  93.8 2.2 copy-start.2
  96.4 2.5 copy-start.4
  98.8 32.1 %copy-start.23 = (f32[8]{0:T(128)S(1)}, f32[8]{0:T(128)}, u32[]{:S(2)}) copy-start(f32[8]{0:T(128)} %get-tuple-element.108) | copy-start | bytes 100
  98.8 32.1 %copy-start.24 = (f32[8]{0:T(128)S(1)}, f32[8]{0:T(128)}, u32[]{:S(2)}) copy-start(f32[8]{0:T(128)} %get-tuple-element.109) | copy-start | bytes 100
  98.8 32.1 %copy-start.25 = (f32[8]{0:T(128)S(1)}, f32[8]{0:T(128)}, u32[]{:S(2)}) copy-start(f32[8]{0:T(128)} %get-tuple-element.110) | copy-start | bytes 100
  98.8 32.1 %copy-start.26 = (f32[8]{0:T(128)S(1)}, f32[8]{0:T(128)}, u32[]{:S(2)}) copy-start(f32[8]{0:T(128)} %get-tuple-element.111) | copy-start | bytes 100
  118.0 26.4 %copy-start.6 = (bf16[1024,1,1,128]{3,0,2,1:T(8,128)(2,1)S(1)}, bf16[1024,1,1,128]{3,0,2,1:T(8,128)(2,1)}, u32[]{:S(2)}) copy-start(bf16[1024,1,1,128]{3,0,2,1:T(8,128)(2,1)} %copy.54) | copy-start | bytes 786436
  118.0 26.3 %copy-start.9 = (bf16[8,1,8,64,128]{4,3,2,1,0:T(8,128)(2,1)S(1)}, bf16[8,1,8,64,128]{4,3,2,1,0:T(8,128)(2,1)}, u32[]{:S(2)}) copy-start(bf16[8,1,8,64,128]{4,3,2,1,0:T(8,128)(2,1)} %get-tuple-element.33) | copy-start | bytes 3145732
  131.2 13.6 %copy-start.5 = (bf16[64,8,8,128]{3,2,1,0:T(8,128)(2,1)S(1)}, bf16[64,8,8,128]{3,2,1,0:T(8,128)(2,1)}, u32[]{:S(2)}) copy-start(bf16[64,8,8,128]{3,2,1,0:T(8,128)(2,1)} %copy-done.4) | copy-start | bytes 3145732
  131.2 13.6 %copy-start.10 = (f32[8,128,128]{2,1,0:T(8,128)S(1)}, f32[8,128,128]{2,1,0:T(8,128)}, u32[]{:S(2)}) copy-start(f32[8,128,128]{2,1,0:T(8,128)} %fusion.108) | copy-start | bytes 1572868
  131.2 13.6 %copy-start.17 = (f32[8,8,128]{2,1,0:T(8,128)S(1)}, f32[8,8,128]{2,1,0:T(8,128)}, u32[]{:S(2)}) copy-start(f32[8,8,128]{2,1,0:T(8,128)} %copy.57) | copy-start | bytes 98308
  131.2 13.6 %copy-start.18 = (f32[8,8,128]{2,1,0:T(8,128)S(1)}, f32[8,8,128]{2,1,0:T(8,128)}, u32[]{:S(2)}) copy-start(f32[8,8,128]{2,1,0:T(8,128)} %get-tuple-element.92) | copy-start | bytes 98308
  131.2 13.6 %copy-start.19 = (pred[128,128]{1,0:T(8,128)(4,1)S(1)}, pred[128,128]{1,0:T(8,128)(4,1)}, u32[]{:S(2)}) copy-start(pred[128,128]{1,0:T(8,128)(4,1)} %iota_compare_fusion) | copy-start | bytes 49156
  144.8 1.7 copy-start.14
  144.8 1.7 copy-start.15
  144.8 1.7 copy-start.27
  144.8 1.7 copy-start.28
  144.8 1.7 copy-start.29
  144.9 1.7 copy-start.30
  149.1 2.9 copy-start.34
  156.5 235.9 %all-gather.6.cloned.1.call-start = ((), (), s32[]{:S(2)}) async-start(), calls=%async_computation.1 | async-start | bytes 9191424 | tf_op jit(solution)/shard_map/all_gather | solution.py:16
  158.4 291.6 %reduce-scatter.2.cloned.1.call-start = ((), (), s32[]{:S(2)}) async-start(), calls=%async_computation.2 | async-start | bytes 4718592 | tf_op jit(solution)/shard_map/reduce_scatter | solution.py:214
  324.7 67.6 %copy-start.33 = (f32[2048]{0:T(1024)S(1)}, f32[2048]{0:T(1024)}, u32[]{:S(2)}) copy-start(f32[2048]{0:T(1024)} %param.32) | copy-start | bytes 24580
  412.7 39.4 %copy-start.1 = (bf16[512,2048]{1,0:T(8,128)(2,1)S(1)}, bf16[512,2048]{1,0:T(8,128)(2,1)}, u32[]{:S(2)}) copy-start(bf16[512,2048]{1,0:T(8,128)(2,1)} %param.31) | copy-start | bytes 6291460
  (9 other events, 10.4 us)
Sparse Core Ops, SparseCore 0:
  156.6 153.8 all-gather.7
  312.7 79.6 all-gather.5
  412.9 37.0 reduce-scatter.1
